TPU v7x, 32 devices: a whole 2x2x4 slice. The times are simulated.
32 devices in a mesh: sp: 8 (over z, y), tp: 4 (over x, core).
Axes of the slice: x: 2, y: 2, z: 4, core: 2. Of those that a mesh axis runs over, the one named last changes fastest.
Arguments:
- query_first: bfloat16 [2048, 512], P('sp', 'tp'), may hold values from -6 to 6
- key_first: bfloat16 [2048, 512], P('sp', 'tp'), may hold values from -6 to 6
- value_first: bfloat16 [2048, 1024], P('sp', 'tp'), may hold values from -6 to 6
- decay_first: float32 [2048, 512], P('sp', 'tp'), may hold values from -1 to 0
- gate_first: bfloat16 [2048, 1024], P('sp', 'tp'), may hold values from -6 to 6
- norm_first: float32 [256], replicated, may hold values from 0.1 to 1.9
- proj_first: bfloat16 [1024, 2048], P('tp', 'sp'), may hold values from -0.125 to 0.125
- query_second: bfloat16 [2048, 512], P('sp', 'tp'), may hold values from -6 to 6
- key_second: bfloat16 [2048, 512], P('sp', 'tp'), may hold values from -6 to 6
- value_second: bfloat16 [2048, 1024], P('sp', 'tp'), may hold values from -6 to 6
- decay_second: float32 [2048, 512], P('sp', 'tp'), may hold values from -1 to 0
- gate_second: bfloat16 [2048, 1024], P('sp', 'tp'), may hold values from -6 to 6
- norm_second: float32 [128], replicated, may hold values from 0.1 to 1.9
- proj_second: bfloat16 [1024, 2048], P('tp', 'sp'), may hold values from -0.125 to 0.125
- residual_in: bfloat16 [2048, 2048], P(('sp', 'tp')), may hold values from -6 to 6
- expert_norm: float32 [2048], replicated, may hold values from 0.1 to 1.9
- route_ids: int32 [2048, 2], P('sp'), may hold values from 0 to 7, all different within a row; in each aligned block of 256 rows (0 to 255, 256 to 511, ...) at most 128 rows name the same one
- route_weight: float32 [2048, 2], P('sp'), may hold values from 0.1 to 0.9
- expert_gate: bfloat16 [8, 2048, 3584], P('sp', None, 'tp'), may hold values from -0.125 to 0.125
- expert_up: bfloat16 [8, 2048, 3584], P('sp', None, 'tp'), may hold values from -0.125 to 0.125
- expert_down: bfloat16 [8, 3584, 2048], P('sp', 'tp'), may hold values from -0.09375 to 0.09375
Outputs:
- layer_out: bfloat16 [2048, 2048], P(('sp', 'tp'))
Inputs may be any that keep to these rules, and one draw needn't show every extreme that they name: `route_ids`: each row names 2 different experts. Among the 256 rows of one index of sp no expert is named by more than 128 rows, and in every draw some expert is named by exactly 128 of them.
All inputs are finite; a program needn't handle non-finite values.
Results may differ from a plain program's by a relative error of at most 0.015.
Values may be sent and summed in bfloat16 or wider, within the bound.
A program may use at most 64 MiB of HBM per device.

v0:
```python
import jax
import jax.numpy as jnp
from jax import lax
from jax.sharding import PartitionSpec as P

KA = 128
VA = 256
KB = 64
VB = 128
BLK = 64


epsilon = 1e-06
highest = lax.Precision.HIGHEST


def entering(value, axis, combine, identity):
    size, index = (lax.axis_size(axis), lax.axis_index(axis))
    everything = jax.tree.map(
        lambda part, kind: lax.all_gather(part.astype(kind), axis),
        value,
        (jnp.bfloat16, jnp.bfloat16, jnp.bfloat16, jnp.bfloat16),
    )
    start = jax.tree.map(
        lambda part, zero: jnp.broadcast_to(jnp.asarray(zero, part.dtype), part.shape),
        value,
        identity,
    )

    def step(k, before):
        reached = k < index
        new = combine(
            before, jax.tree.map(lambda part, own: part[k].astype(own.dtype), everything, value)
        )
        return jax.tree.map(lambda a, b: jnp.where(reached, a, b), new, before)

    return lax.fori_loop(0, size, step, start)


def local_pass(queries, key_rows, values, decay_factors, key_width, value_width):
    count_of_tokens = queries.shape[0]
    head_count = queries.shape[1] // key_width
    blocks = count_of_tokens // BLK

    def arrange(source, feature_channels):
        return (
            source.astype(jnp.float32)
            .reshape(blocks, BLK, head_count, feature_channels)
            .transpose(0, 2, 1, 3)
        )

    causal = jnp.tril(jnp.ones((BLK, BLK), jnp.float32))

    def block_step(carry_state, inputs):
        query_block, key_block, value_block, decay_block = inputs
        cumulative = jnp.cumsum(decay_block, axis=1)
        block_end = cumulative[:, -1:, :]
        query_decayed = query_block * jnp.exp(cumulative)
        key_inverse = key_block * jnp.exp(-cumulative)
        key_to_end = key_block * jnp.exp(block_end - cumulative)
        scores = jnp.einsum("htd,hsd->hts", query_decayed, key_inverse, precision=highest) * causal
        outputs = jnp.einsum("hts,hsv->htv", scores, value_block, precision=highest)
        outputs = outputs + jnp.einsum(
            "htd,hdv->htv", query_decayed, carry_state, precision=highest
        )
        carry_state = jnp.exp(block_end)[:, 0, :, None] * carry_state + jnp.einsum(
            "hsd,hsv->hdv", key_to_end, value_block, precision=highest
        )
        return (carry_state, outputs)

    start_state = jnp.zeros((head_count, key_width, value_width), jnp.float32)
    scaled = arrange(queries, key_width) * key_width ** (-0.5)
    end_state, outputs = lax.scan(
        block_step,
        start_state,
        (
            scaled,
            arrange(key_rows, key_width),
            arrange(values, value_width),
            arrange(decay_factors, key_width),
        ),
    )
    local_out = outputs.transpose(0, 2, 1, 3).reshape(count_of_tokens, head_count, value_width)
    running = jnp.cumsum(decay_factors.reshape(count_of_tokens, head_count, key_width), axis=0)
    readout = queries.astype(jnp.float32).reshape(
        count_of_tokens, head_count, key_width
    ) * key_width ** (-0.5)
    readout = readout * jnp.exp(running)
    return (local_out, readout, running[-1], end_state)


def chain_step(earlier, latter):
    return (
        earlier[0] + latter[0],
        jnp.exp(latter[0])[:, :, None] * earlier[1] + latter[1],
        earlier[2] + latter[2],
        jnp.exp(latter[2])[:, :, None] * earlier[3] + latter[3],
    )


def head_norm(attention, head_gain, gate):
    inverse_rms = lax.rsqrt(jnp.mean(attention * attention, axis=-1, keepdims=True) + epsilon)
    gate_silu = jax.nn.silu(gate.astype(jnp.float32).reshape(attention.shape))
    mixed_rows = attention * inverse_rms * head_gain * gate_silu
    return mixed_rows.astype(jnp.bfloat16).reshape(attention.shape[0], -1)


def rms_scale(residual, gain_vector):
    as_float = residual.astype(jnp.float32)
    inverse_rms = lax.rsqrt(jnp.mean(as_float * as_float, axis=-1, keepdims=True) + epsilon)
    return (as_float * inverse_rms * gain_vector).astype(jnp.bfloat16)


def route_tables(block_routes, experts, capacity):
    block_tokens, top_count = block_routes.shape
    flattened = block_routes.reshape(-1)
    onehot = (flattened[:, None] == jnp.arange(experts, dtype=jnp.int32)[None, :]).astype(jnp.int32)
    before = jnp.cumsum(onehot, axis=0) - onehot
    ranking = jnp.sum(before * onehot, axis=1)
    slot_ids = flattened * capacity + ranking
    row_token = jnp.arange(block_tokens * top_count, dtype=jnp.int32) // top_count
    owners = jnp.full((experts * capacity,), block_tokens, jnp.int32).at[slot_ids].set(row_token)
    return (owners, slot_ids)


def expert_rows(incoming, gate_matrix, up_matrix, down_matrix):
    flattened = incoming.reshape(-1, incoming.shape[-1])
    gate_part = jnp.dot(flattened, gate_matrix, preferred_element_type=jnp.float32)
    up_part = jnp.dot(flattened, up_matrix, preferred_element_type=jnp.float32)
    hidden = (jax.nn.silu(gate_part) * up_part).astype(jnp.bfloat16)
    return jnp.dot(hidden, down_matrix, preferred_element_type=jnp.float32).reshape(incoming.shape)


def shards(
    query_first,
    key_first,
    value_first,
    decay_first,
    gate_first,
    norm_first,
    proj_first,
    query_second,
    key_second,
    value_second,
    decay_second,
    gate_second,
    norm_second,
    proj_second,
    residual_in,
    expert_norm,
    route_ids,
    route_weight,
    expert_gate,
    expert_up,
    expert_down,
):
    local_first, readout_first, total_first, state_first = local_pass(
        query_first, key_first, value_first, decay_first, KA, VA
    )
    local_second, readout_second, total_second, state_second = local_pass(
        query_second, key_second, value_second, decay_second, KB, VB
    )
    identity = (
        jnp.zeros_like(total_first),
        jnp.zeros_like(state_first),
        jnp.zeros_like(total_second),
        jnp.zeros_like(state_second),
    )
    carried = entering(
        (total_first, state_first, total_second, state_second), "sp", chain_step, identity
    )
    attention_first = local_first + jnp.einsum(
        "thd,hdv->thv", readout_first, carried[1], precision=highest
    )
    attention_second = local_second + jnp.einsum(
        "thd,hdv->thv", readout_second, carried[3], precision=highest
    )
    mixed_first = head_norm(attention_first, norm_first, gate_first)
    mixed_second = head_norm(attention_second, norm_second, gate_second)
    mixed_rows = jnp.concatenate((mixed_first, mixed_second), axis=1)
    projection = jnp.concatenate((proj_first, proj_second), axis=0)
    partial_terms = jnp.dot(
        mixed_rows,
        lax.all_gather(projection, "sp", axis=1, tiled=True),
        preferred_element_type=jnp.float32,
    )
    mixture = lax.psum_scatter(
        partial_terms.astype(jnp.bfloat16), "tp", scatter_dimension=0, tiled=True
    ).astype(jnp.float32)
    residual = (residual_in.astype(jnp.float32) + mixture).astype(jnp.bfloat16)
    normed = rms_scale(residual, expert_norm)
    gathered = lax.all_gather(normed, "tp", axis=0, tiled=True)
    block_tokens, top_count = route_ids.shape
    model_width = gathered.shape[1]
    experts = lax.axis_size("sp")
    capacity = 2 * top_count * block_tokens // experts
    owners, slot_ids = route_tables(route_ids, experts, capacity)
    padded = jnp.concatenate((gathered, jnp.zeros((1, model_width), jnp.bfloat16)), axis=0)
    outgoing = jnp.take(padded, owners, axis=0).reshape(experts, capacity, model_width)
    gate_matrix = expert_gate[0]
    up_matrix = expert_up[0]
    down_matrix = expert_down[0]
    quarter = capacity // lax.axis_size("tp")
    tp_index = lax.axis_index("tp")
    own_slots = lax.dynamic_slice_in_dim(outgoing, tp_index * quarter, quarter, 1)
    whole_slots = lax.all_gather(
        lax.all_to_all(own_slots, "sp", split_axis=0, concat_axis=0, tiled=True),
        "tp",
        axis=1,
        tiled=True,
    )
    produced = expert_rows(whole_slots, gate_matrix, up_matrix, down_matrix)
    summed = lax.psum_scatter(
        produced.astype(jnp.bfloat16), "tp", scatter_dimension=1, tiled=True
    ).astype(jnp.float32)
    returned = lax.all_to_all(
        summed.astype(jnp.bfloat16), "sp", split_axis=0, concat_axis=0, tiled=True
    ).astype(summed.dtype)
    position = slot_ids % capacity
    expert_of = slot_ids // capacity
    inside = position // quarter == tp_index
    local_index = jnp.where(
        inside, expert_of * quarter + position - tp_index * quarter, experts * quarter
    )
    flat_back = jnp.concatenate(
        (
            returned.reshape(experts * quarter, model_width),
            jnp.zeros((1, model_width), jnp.float32),
        ),
        axis=0,
    )
    picked = jnp.take(flat_back, local_index, axis=0)
    weighted = (
        (picked * route_weight.reshape(-1, 1))
        .reshape(block_tokens, top_count, model_width)
        .sum(axis=1)
    )
    combined = lax.psum_scatter(
        weighted.astype(jnp.bfloat16), "tp", scatter_dimension=0, tiled=True
    ).astype(jnp.float32)
    return (residual.astype(jnp.float32) + combined).astype(jnp.bfloat16)


def solution(mesh):
    in_specs = (
        P("sp", "tp"),
        P("sp", "tp"),
        P("sp", "tp"),
        P("sp", "tp"),
        P("sp", "tp"),
        P(),
        P("tp", "sp"),
        P("sp", "tp"),
        P("sp", "tp"),
        P("sp", "tp"),
        P("sp", "tp"),
        P("sp", "tp"),
        P(),
        P("tp", "sp"),
        P(("sp", "tp"), None),
        P(),
        P("sp", None),
        P("sp", None),
        P("sp", None, "tp"),
        P("sp", None, "tp"),
        P("sp", "tp", None),
    )
    out_specs = P(("sp", "tp"), None)
    return jax.shard_map(shards, mesh=mesh, in_specs=in_specs, out_specs=out_specs, check_vma=False)
```

profile of v0, /device:TPU:13, one launch (start us, length us, event | category | flops | bytes accessed | tf_op | source)
XLA Modules:
  0.0 396.7 jit_solution(9344784152985778146)
XLA Ops:
  6.5 1.7 pad_maximum_fusion
  8.3 1.0 fusion.95
  9.4 1.0 copy.64
  10.4 1.1 reshape.560
  11.6 1.2 reduce-window.24
  13.4 11.5 %all_gather.32 = bf16[8,2,64]{2,1,0:T(2,128)(2,1)S(1)} all-gather(bf16[1,2,64]{2,1,0:T(2,128)(2,1)S(1)} %copy.69), channel_id=1, replica_groups=mesh['sp'=8,'tp'=4] {'sp'}, dimensions={0}, use_global_device_ids=true | all-gather | bytes 2304 | tf_op jit(solution)/shard_map/all_gather | solution.py:20
  24.9 16.3 %all_gather.29 = bf16[8,1,128]{2,1,0:T(2,128)(2,1)S(1)} all-gather(bf16[1,1,128]{2,1,0:T(2,128)(2,1)S(1)} %slice_bitcast_fusion.3), channel_id=1, replica_groups=mesh['sp'=8,'tp'=4] {'sp'}, dimensions={0}, use_global_device_ids=true | all-gather | bytes 2304 | tf_op jit(solution)/shard_map/all_gather | solution.py:20
  42.1 4.8 %while.43 = (s32[]{:T(128)}, f32[2,64,128]{2,1,0:T(8,128)S(1)}, f32[4,2,64,128]{3,2,0,1:T(8,128)S(1)}, f32[4,2,64,64]{3,1,2,0:T(2,128)S(1)}, f32[4,2,64,64]{3,1,...) while((s32[]{:T(128)}, f32[2,64,128]{2,1,0:T(8,128)S(1)}, ...), condition=%wide.region_9.10_spmd.clone, body=%wide.region_7.9_spmd.clone.sunk | while | flops 44703744 | bytes 1378948 | solution.py:73
  42.3 0.2 convolution_multiply_fusion.5
  42.8 0.2 fusion.163
  43.0 0.3 convolution_add_fusion.4
  43.5 0.2 convolution_multiply_fusion.5
  44.0 0.2 fusion.163
  44.2 0.3 convolution_add_fusion.4
  44.7 0.2 convolution_multiply_fusion.5
  45.2 0.2 fusion.163
  45.4 0.3 convolution_add_fusion.4
  45.9 0.2 convolution_multiply_fusion.5
  46.4 0.2 fusion.163
  46.6 0.3 convolution_add_fusion.4
  47.0 22.8 %all-gather.1 = bf16[16,64,128]{2,1,0:T(8,128)(2,1)S(1)} all-gather(bf16[2,64,128]{2,1,0:T(8,128)(2,1)S(1)} %convert_element_type.136), channel_id=3, replica_groups=mesh['sp'=8,'tp'=4] {'sp'}, dimensions={0}, use_global_device_ids=true | all-gather | bytes 294912 | tf_op jit(solution)/shard_map/all_gather | solution.py:20
  69.9 7.7 %while.42 = (s32[]{:T(128)}, f32[1,128,256]{2,1,0:T(8,128)S(1)}, f32[4,1,64,256]{3,2,1,0:T(8,128)S(1)}, f32[4,1,64,128]{3,2,1,0:T(8,128)}, f32[4,1,64,128]{3,2,1...) while((s32[]{:T(128)}, f32[1,128,256]{2,1,0:T(8,128)S(1)}, ...), condition=%wide.region_2.3_spmd.clone, body=%wide.region_0.2_spmd.clone.sunk | while | flops 69931008 | bytes 1169020 | solution.py:73
  69.9 0.8 dynamic-slice_bitcast_fusion.2
  71.2 0.2 fusion.154
  71.5 0.4 fusion.152
  71.9 0.8 dynamic-slice_bitcast_fusion.2
  73.1 0.2 fusion.154
  73.4 0.4 fusion.152
  73.8 0.8 dynamic-slice_bitcast_fusion.2
  75.0 0.2 fusion.154
  75.3 0.4 fusion.152
  75.7 0.8 dynamic-slice_bitcast_fusion.2
  77.2 0.4 fusion.152
  77.6 25.3 %all-gather = bf16[8,128,256]{2,1,0:T(8,128)(2,1)S(1)} all-gather(bf16[1,128,256]{2,1,0:T(8,128)(2,1)S(1)} %convert_element_type.134), channel_id=2, replica_groups=mesh['sp'=8,'tp'=4] {'sp'}, dimensions={0}, use_global_device_ids=true | all-gather | bytes 589824 | tf_op jit(solution)/shard_map/all_gather | solution.py:20
  102.9 2.1 while.44
  105.5 0.4 multiply_reduce_fusion.2
  106.0 0.4 multiply_reduce_fusion.1
  106.7 3.3 convolution_convert_fusion.1
  110.6 46.7 %reduce-scatter.4.cloned.1.call-done = bf16[64,2048]{1,0:T(8,128)(2,1)} async-done(((bf16[256,2048]{1,0:T(8,128)(2,1)}), bf16[64,2048]{1,0:T(8,128)(2,1)}) %reduce-scatter.4.cloned.1.call-update) | async-done | bytes 262160 | tf_op jit(solution)/shard_map/reduce_scatter | solution.py:187
  157.2 1.1 fusion.69
  158.4 1.8 fusion.71
  160.3 1.1 reduce-window.26
  162.0 2.4 scatter_custom_fusion
  164.5 13.1 %all-gather.8.cloned.1.call-done = bf16[256,2048]{1,0:T(8,128)(2,1)} async-done(((bf16[64,2048]{1,0:T(8,128)(2,1)}), bf16[256,2048]{1,0:T(8,128)(2,1)}) %all-gather.8.cloned.1.call-update) | async-done | bytes 1048592 | tf_op jit(solution)/shard_map/all_gather | solution.py:192
  177.6 1.3 concatenate.16
  178.9 6.0 %gather_fusion = bf16[1024,2048]{1,0:T(8,128)(2,1)} fusion(bf16[257,2048]{1,0:T(8,128)(2,1)S(1)} %concatenate.16, s32[1024]{0:T(1024)S(1)} %fusion.106), kind=kCustom, calls=%fused_computation | custom fusion | bytes 8392704 | tf_op jit(solution)/shard_map/jit(_take)/gather | solution.py:199
  184.9 1.5 dynamic-slice_select_fusion
  186.4 28.1 %all_to_all.10 = bf16[8,32,2048]{2,1,0:T(8,128)(2,1)} all-to-all(bf16[8,32,2048]{2,1,0:T(8,128)(2,1)S(1)} %dynamic-slice_select_fusion), channel_id=1, replica_groups=mesh['sp'=8,'tp'=4] {'sp'}, dimensions={0} | all-to-all | bytes 2097152 | tf_op jit(solution)/shard_map/all_to_all | solution.py:207
  214.6 0.2 reduce-scatter.6.cloned.1.call-start
  214.8 35.9 %all-gather.10.cloned.1.call-done = bf16[8,128,2048]{2,1,0:T(8,128)(2,1)} async-done(((bf16[8,32,2048]{2,1,0:T(8,128)(2,1)}), bf16[8,128,2048]{2,1,0:T(8,128)(2,1)}) %all-gather.10.cloned.1.call-update) | async-done | bytes 4194320 | tf_op jit(solution)/shard_map/all_gather | solution.py:206
  250.7 7.5 %fusion.61 = f32[1024,896]{1,0:T(8,128)S(1)} fusion(bf16[1024,2048]{1,0:T(8,128)(2,1)} %bitcast.346, bf16[1,2048,896]{2,1,0:T(8,128)(2,1)} %param.46), kind=kOutput, calls=%fused_computation.86 | convolution fusion | flops 3758096384 | bytes 11534336 | tf_op jit(solution)/shard_map/dot_general | solution.py:129
  258.3 4.7 %multiply_convert_fusion = bf16[1024,896]{1,0:T(8,128)(2,1)S(1)} fusion(f32[1024,896]{1,0:T(8,128)S(1)} %fusion.61, bf16[1024,2048]{1,0:T(8,128)(2,1)S(1)} %bitcast.347, bf16[1,2048,896]{2,1,0:T(8,128)(2,1)S(1)} %copy-done.17), kind=kOutput, calls=%fused_computation.90 | convolution fusion | flops 3763601408 | bytes 13369344 | tf_op jit(solution)/shard_map/dot_general | solution.py:128
  263.0 6.1 %convolution_convert_fusion = bf16[8,128,2048]{2,1,0:T(8,128)(2,1)} fusion(bf16[8,128,896]{2,1,0:T(8,128)(2,1)S(1)} %bitcast.348, bf16[1,896,2048]{2,1,0:T(8,128)(2,1)S(1)} %copy-done.18), kind=kOutput, calls=%fused_computation.84 | convolution fusion | flops 3760193536 | bytes 9699328 | tf_op jit(solution)/shard_map/dot_general | solution.py:131
  269.1 44.2 %reduce-scatter.6.cloned.1.call-done = bf16[8,32,2048]{2,1,0:T(8,128)(2,1)} async-done(((bf16[8,128,2048]{2,1,0:T(8,128)(2,1)}), bf16[8,32,2048]{2,1,0:T(8,128)(2,1)}) %reduce-scatter.6.cloned.1.call-update) | async-done | bytes 1048592 | tf_op jit(solution)/shard_map/reduce_scatter | solution.py:213
  313.3 5.5 %all-to-all-start.1 = ((bf16[8,32,2048]{2,1,0:T(8,128)(2,1)}), bf16[8,32,2048]{2,1,0:T(8,128)(2,1)S(1)}, u32[]{:S(2)}, u32[]{:S(2)}) async-start(bf16[8,32,2048]{2,1,0:T(8,128)(2,1)} %reduce-scatter.6.cloned.1.call-done), calls=%async_computation.3 | async-start | bytes 2097152 | tf_op jit(solution)/shard_map/all_to_all | solution.py:216
  318.9 0.8 copy.86
  319.8 0.3 compare_and_fusion
  320.0 22.0 %all-to-all-done.1 = bf16[8,32,2048]{2,1,0:T(8,128)(2,1)S(1)} async-done(((bf16[8,32,2048]{2,1,0:T(8,128)(2,1)}), bf16[8,32,2048]{2,1,0:T(8,128)(2,1)S(1)}, u32[]{:S(2)}, u32[]{:S(2)}) %all-to-all-start.1) | async-done | bytes 1048608 | tf_op jit(solution)/shard_map/all_to_all | solution.py:216
  342.0 0.2 pad_convert_fusion
  342.2 3.6 gather_fusion.1
  345.9 5.9 %gather.15 = f32[256,2,2048]{2,1,0:T(2,128)} reshape(f32[512,2048]{1,0:T(8,128)} %gather_fusion.1) | data formatting | bytes 8388608 | tf_op jit(solution)/shard_map/jit(_take)/gather | solution.py:232
  351.7 10.9 %multiply_reduce_fusion = bf16[256,2048]{1,0:T(8,128)(2,1)} fusion(f32[256,2,2048]{2,1,0:T(2,128)} %gather.15, pred[256,2]{1,0:T(8,128)(4,1)S(1)} %compare_and_fusion, f32[256,2]{1,0:T(8,128)S(1)} %copy-done.2), kind=kLoop, calls=%fused_computation.83 | loop fusion | flops 2621440 | bytes 5245440 | tf_op jit(solution)/shard_map/reduce_sum | solution.py:236
  362.7 25.5 %reduce-scatter.8.cloned.1.call-done = bf16[64,2048]{1,0:T(8,128)(2,1)} async-done(((bf16[256,2048]{1,0:T(8,128)(2,1)}), bf16[64,2048]{1,0:T(8,128)(2,1)}) %reduce-scatter.8.cloned.1.call-update) | async-done | bytes 262160 | tf_op jit(solution)/shard_map/reduce_scatter | solution.py:238
  388.1 1.7 fusion.72
  (191 shorter events, 9.0 us)
Async XLA Ops:
  6.5 34.8 %copy-start.10 = (bf16[256,128]{1,0:T(8,128)(2,1)S(1)}, bf16[256,128]{1,0:T(8,128)(2,1)}, u32[]{:S(2)}) copy-start(bf16[256,128]{1,0:T(8,128)(2,1)} %param.34) | copy-start | bytes 196612
  6.5 35.2 %copy-start.8 = (bf16[256,128]{1,0:T(8,128)(2,1)S(1)}, bf16[256,128]{1,0:T(8,128)(2,1)}, u32[]{:S(2)}) copy-start(bf16[256,128]{1,0:T(8,128)(2,1)} %param.35) | copy-start | bytes 196612
  6.5 35.4 %copy-start.4 = (bf16[256,256]{1,0:T(8,128)(2,1)S(1)}, bf16[256,256]{1,0:T(8,128)(2,1)}, u32[]{:S(2)}) copy-start(bf16[256,256]{1,0:T(8,128)(2,1)} %param.36) | copy-start | bytes 393220
  6.5 100.2 %all-gather.6.cloned.1.call-start = ((), (), s32[]{:S(2)}) async-start(), calls=%async_computation.5 | async-start | bytes 2359296 | tf_op jit(solution)/shard_map/all_gather | solution.py:184
  8.3 148.9 %reduce-scatter.4.cloned.1.call-start = ((), (), s32[]{:S(2)}) async-start(), calls=%async_computation.6 | async-start | bytes 1310720 | tf_op jit(solution)/shard_map/reduce_scatter | solution.py:187
  42.1 27.7 %copy-start.5 = (bf16[256,256]{1,0:T(8,128)(2,1)S(1)}, bf16[256,256]{1,0:T(8,128)(2,1)}, u32[]{:S(2)}) copy-start(bf16[256,256]{1,0:T(8,128)(2,1)} %param.29) | copy-start | bytes 393220
  42.1 27.7 %copy-start.3 = (bf16[256,128]{1,0:T(8,128)(2,1)S(1)}, bf16[256,128]{1,0:T(8,128)(2,1)}, u32[]{:S(2)}) copy-start(bf16[256,128]{1,0:T(8,128)(2,1)} %param.27) | copy-start | bytes 196612
  42.1 27.8 %copy-start.9 = (bf16[256,128]{1,0:T(8,128)(2,1)S(1)}, bf16[256,128]{1,0:T(8,128)(2,1)}, u32[]{:S(2)}) copy-start(bf16[256,128]{1,0:T(8,128)(2,1)} %param.28) | copy-start | bytes 196612
  69.9 35.3 %copy-start.6 = (bf16[256,256]{1,0:T(8,128)(2,1)S(1)}, bf16[256,256]{1,0:T(8,128)(2,1)}, u32[]{:S(2)}) copy-start(bf16[256,256]{1,0:T(8,128)(2,1)} %param.38) | copy-start | bytes 393220
  77.6 27.8 %copy-start.7 = (bf16[256,256]{1,0:T(8,128)(2,1)S(1)}, bf16[256,256]{1,0:T(8,128)(2,1)}, u32[]{:S(2)}) copy-start(bf16[256,256]{1,0:T(8,128)(2,1)} %param.31) | copy-start | bytes 393220
  77.6 28.9 %copy-start.14 = (f32[256]{0:T(256)S(1)}, f32[256]{0:T(256)}, u32[]{:S(2)}) copy-start(f32[256]{0:T(256)} %param.32) | copy-start | bytes 3076
  77.6 29.0 %copy-start.15 = (f32[128]{0:T(128)S(1)}, f32[128]{0:T(128)}, u32[]{:S(2)}) copy-start(f32[128]{0:T(128)} %param.39) | copy-start | bytes 1540
  105.5 4.6 %copy-start.12 = (s32[256,2]{0,1:T(2,128)S(1)}, s32[256,2]{0,1:T(2,128)}, u32[]{:S(2)}) copy-start(s32[256,2]{0,1:T(2,128)} %param.43) | copy-start | bytes 6148
  106.0 51.3 %copy-start = (bf16[64,2048]{1,0:T(8,128)(2,1)S(1)}, bf16[64,2048]{1,0:T(8,128)(2,1)}, u32[]{:S(2)}) copy-start(bf16[64,2048]{1,0:T(8,128)(2,1)} %param.41) | copy-start | bytes 786436
  106.0 52.4 %copy-start.11 = (f32[2048]{0:T(1024)S(1)}, f32[2048]{0:T(1024)}, u32[]{:S(2)}) copy-start(f32[2048]{0:T(1024)} %param.42) | copy-start | bytes 24580
  110.1 67.6 %all-gather.8.cloned.1.call-start = ((), (), s32[]{:S(2)}) async-start(), calls=%async_computation.7 | async-start | bytes 1310720 | tf_op jit(solution)/shard_map/all_gather | solution.py:192
  160.2 90.5 %all-gather.10.cloned.1.call-start = ((), (), s32[]{:S(2)}) async-start(), calls=%async_computation.8 | async-start | bytes 5242880 | tf_op jit(solution)/shard_map/all_gather | solution.py:206
  214.6 98.7 %reduce-scatter.6.cloned.1.call-start = ((), (), s32[]{:S(2)}) async-start(), calls=%async_computation.9 | async-start | bytes 5242880 | tf_op jit(solution)/shard_map/reduce_scatter | solution.py:213
  250.7 7.5 %copy-start.16 = (bf16[8,128,2048]{2,1,0:T(8,128)(2,1)S(1)}, bf16[8,128,2048]{2,1,0:T(8,128)(2,1)}, u32[]{:S(2)}) copy-start(bf16[8,128,2048]{2,1,0:T(8,128)(2,1)} %all-gather.10.cloned.1.call-done) | copy-start | bytes 12582916
  250.7 7.5 %copy-start.17 = (bf16[1,2048,896]{2,1,0:T(8,128)(2,1)S(1)}, bf16[1,2048,896]{2,1,0:T(8,128)(2,1)}, u32[]{:S(2)}) copy-start(bf16[1,2048,896]{2,1,0:T(8,128)(2,1)} %param.45) | copy-start | bytes 11010052
  258.2 4.8 %copy-start.18 = (bf16[1,896,2048]{2,1,0:T(8,128)(2,1)S(1)}, bf16[1,896,2048]{2,1,0:T(8,128)(2,1)}, u32[]{:S(2)}) copy-start(bf16[1,896,2048]{2,1,0:T(8,128)(2,1)} %param.47) | copy-start | bytes 11010052
  269.1 49.8 %copy-start.13 = (f32[256,2]{0,1:T(2,128)S(1)}, f32[256,2]{0,1:T(2,128)}, u32[]{:S(2)}) copy-start(f32[256,2]{0,1:T(2,128)} %param.44) | copy-start | bytes 6148
  313.3 28.7 %all-to-all-start.1 = ((bf16[8,32,2048]{2,1,0:T(8,128)(2,1)}), bf16[8,32,2048]{2,1,0:T(8,128)(2,1)S(1)}, u32[]{:S(2)}, u32[]{:S(2)}) async-start(bf16[8,32,2048]{2,1,0:T(8,128)(2,1)} %reduce-scatter.6.cloned.1.call-done), calls=%async_computation.3 | async-start | bytes 2097152 | tf_op jit(solution)/shard_map/all_to_all | solution.py:216
  318.8 69.4 %reduce-scatter.8.cloned.1.call-start = ((), (), s32[]{:S(2)}) async-start(), calls=%async_computation.10 | async-start | bytes 1310720 | tf_op jit(solution)/shard_map/reduce_scatter | solution.py:238
  345.9 5.9 %copy-start.2 = (f32[256,2]{1,0:T(8,128)S(1)}, f32[256,2]{1,0:T(8,128)}, u32[]{:S(2)}) copy-start(f32[256,2]{1,0:T(8,128)} %copy.86) | copy-start | bytes 6148
  351.7 36.4 %copy-start.1 = (bf16[64,2048]{1,0:T(8,128)(2,1)S(1)}, bf16[64,2048]{1,0:T(8,128)(2,1)}, u32[]{:S(2)}) copy-start(bf16[64,2048]{1,0:T(8,128)(2,1)} %reduce-scatter.4.cloned.1.call-done) | copy-start | bytes 786436
Sparse Core Ops, SparseCore 0:
  9.4 48.7 all-gather.5
  110.2 47.0 reduce-scatter.3
  160.3 17.2 all-gather.7
  214.7 35.9 all-gather.9
  269.3 43.9 reduce-scatter.5
  362.8 25.3 reduce-scatter.7
where the time goes:
time: 399 us; the launch traced here: 397 us
  waiting for transfers between devices  187 us (47%)
  blocking collectives  104 us (26%)
  matrix products  30.3 us (8%)
  local copies, waits for them, and re-layouts  28.2 us (7%)
  other arithmetic  25.9 us (6%)
  between operations  14.1 us (4%)
  starting transfers between devices  5.83 us (1%)
    all_gather x4, blocking collectives, entering(): lax.all_gather(part.astype(kind), axis)  75.9 us
    reduce_scatter x1, waiting for transfers between devices, shards(): lax.psum_scatter(partial_terms.astype(jnp.bfloat16), 'tp', scatter_dimens...  46.7 us
    reduce_scatter x1, waiting for transfers between devices, shards(): lax.psum_scatter(produced.astype(jnp.bfloat16), 'tp', scatter_dimension=1...  44.2 us
    all_gather x1, waiting for transfers between devices, shards(): lax.all_gather(lax.all_to_all(own_slots, 'sp', split_axis=0, concat_axis=...  35.9 us
    all_to_all x1, blocking collectives, shards(): lax.all_to_all(own_slots, 'sp', split_axis=0, concat_axis=0, tiled=True)  28.1 us
    reduce_scatter x1, waiting for transfers between devices, shards(): lax.psum_scatter(weighted.astype(jnp.bfloat16), 'tp', scatter_dimension=0...  25.5 us
    all_to_all x1, waiting for transfers between devices, shards(): lax.all_to_all(summed.astype(jnp.bfloat16), 'sp', split_axis=0, concat_ax...  22 us
    all_gather x1, waiting for transfers between devices, shards(): gathered = lax.all_gather(normed, 'tp', axis=0, tiled=True)  13.1 us
  transfers between devices with their start and end apart: 7, of which 6 were waited for; matrix products, arithmetic and copies ran while one was open for 7% of the time, Pallas kernels for 0%

commit v1 on v0

v1 whole, which is shorter than its diff:
```python
import functools

import jax
import jax.numpy as jnp
from jax import lax
from jax.experimental import pallas as pl
from jax.experimental.pallas import tpu as pltpu
from jax.sharding import PartitionSpec as P

KA = 128
VA = 256
KB = 64
VB = 128
BLK = 64
PAIR = 2


epsilon = 1e-06
highest = lax.Precision.HIGHEST
MESH = pl.DeviceIdType.MESH
VMEM = pl.BlockSpec(memory_space=pltpu.VMEM)


def greet(peers):
    barrier = pltpu.get_barrier_semaphore()
    for peer in peers:
        pl.semaphore_signal(barrier, inc=1, device_id=peer, device_id_type=MESH)
    pl.semaphore_wait(barrier, len(peers))


def group_member(axis, span, step):
    me = lax.axis_index(axis)
    inside = lax.rem(me, span)
    other = lax.rem(inside + step, span)
    return inside, other, {axis: me - inside + other}


def exchange_kernel(axis, span, spread, count, *refs):
    sources, targets = refs[:count], refs[count : 2 * count]
    send_sems, recv_sems = refs[2 * count :]
    greet([group_member(axis, span, step)[2] for step in range(1, span)])
    copies = []
    for step in range(1, span):
        inside, other, device = group_member(axis, span, step)
        for i in range(count):
            copy = pltpu.make_async_remote_copy(
                src_ref=sources[i].at[other] if spread else sources[i],
                dst_ref=targets[i].at[inside],
                send_sem=send_sems.at[i, step],
                recv_sem=recv_sems.at[i, step],
                device_id=device,
                device_id_type=MESH,
            )
            copy.start()
            copies.append(copy)
    inside = lax.rem(lax.axis_index(axis), span)
    for i in range(count):
        targets[i][inside] = sources[i][inside] if spread else sources[i][...]
    for copy in copies:
        copy.wait()


def exchange(arrays, axis, span, spread, number):
    shapes = tuple(
        jax.ShapeDtypeStruct(a.shape if spread else (span,) + a.shape, a.dtype) for a in arrays
    )
    count = len(arrays)
    return pl.pallas_call(
        functools.partial(exchange_kernel, axis, span, spread, count),
        out_shape=shapes,
        in_specs=[VMEM] * count,
        out_specs=(VMEM,) * count,
        scratch_shapes=[
            pltpu.SemaphoreType.DMA((count, span)),
            pltpu.SemaphoreType.DMA((count, span)),
        ],
        compiler_params=pltpu.CompilerParams(collective_id=number, has_side_effects=True),
    )(*arrays)


def dispatch_kernel(size, source, target, send_sems, recv_sems, pair_send, pair_recv):
    half = lax.rem(lax.axis_index("tp"), PAIR)
    sibling = group_member("tp", PAIR, 1)[2]
    peers = [group_member("sp", size, step) for step in range(1, size)]
    greet([peer[2] for peer in peers] + [sibling])
    copies, forwards = [], []
    for step, (me, other, device) in enumerate(peers, 1):
        copy = pltpu.make_async_remote_copy(
            src_ref=source.at[other],
            dst_ref=target.at[half, me],
            send_sem=send_sems.at[step],
            recv_sem=recv_sems.at[step],
            device_id=device,
            device_id_type=MESH,
        )
        copy.start()
        copies.append(copy)
    me = lax.axis_index("sp")
    own = pltpu.make_async_remote_copy(
        src_ref=source.at[me],
        dst_ref=target.at[half, me],
        send_sem=pair_send.at[0],
        recv_sem=pair_recv.at[0],
        device_id=sibling,
        device_id_type=MESH,
    )
    own.start()
    forwards.append(own)
    target[half, me] = source[me]
    for step in range(1, size):
        copies[step - 1].wait_recv()
        origin = lax.rem(me - step + size, size)
        forward = pltpu.make_async_remote_copy(
            src_ref=target.at[half, origin],
            dst_ref=target.at[half, origin],
            send_sem=pair_send.at[step],
            recv_sem=pair_recv.at[step],
            device_id=sibling,
            device_id_type=MESH,
        )
        forward.start()
        forwards.append(forward)
    for copy in copies:
        copy.wait_send()
    for forward in forwards:
        forward.wait()


def dispatch(outgoing, number):
    size = outgoing.shape[0]
    return pl.pallas_call(
        functools.partial(dispatch_kernel, size),
        out_shape=jax.ShapeDtypeStruct((PAIR,) + outgoing.shape, outgoing.dtype),
        in_specs=[VMEM],
        out_specs=VMEM,
        scratch_shapes=[pltpu.SemaphoreType.DMA((size,)) for _ in range(4)],
        compiler_params=pltpu.CompilerParams(collective_id=number, has_side_effects=True),
    )(outgoing)


def local_pass(queries, key_rows, values, decay_factors, key_width, value_width):
    count_of_tokens = queries.shape[0]
    head_count = queries.shape[1] // key_width
    blocks = count_of_tokens // BLK
    lower = jnp.tril(jnp.ones((BLK, BLK), jnp.float32))

    def arrange(source, feature_channels):
        return (
            source.astype(jnp.float32)
            .reshape(blocks, BLK, head_count, feature_channels)
            .transpose(0, 2, 1, 3)
        )

    query_blocks = arrange(queries, key_width) * key_width ** (-0.5)
    key_blocks = arrange(key_rows, key_width)
    value_blocks = arrange(values, value_width)
    cumulative = jnp.einsum("ts,nhsd->nhtd", lower, arrange(decay_factors, key_width), precision=highest)
    block_end = cumulative[:, :, -1:, :]
    query_decayed = query_blocks * jnp.exp(cumulative)
    key_inverse = key_blocks * jnp.exp(-cumulative)
    key_to_end = key_blocks * jnp.exp(block_end - cumulative)
    scores = jnp.einsum("nhtd,nhsd->nhts", query_decayed, key_inverse, precision=highest) * lower
    inner = jnp.einsum("nhts,nhsv->nhtv", scores, value_blocks, precision=highest)
    added = jnp.einsum("nhsd,nhsv->nhdv", key_to_end, value_blocks, precision=highest)
    state = jnp.zeros((head_count, key_width, value_width), jnp.float32)
    states = []
    for n in range(blocks):
        states.append(state)
        state = jnp.exp(block_end[n, :, 0])[:, :, None] * state + added[n]
    ends = block_end[:, :, 0]
    return (query_decayed, inner, jnp.stack(states), ends, state)


def finish_pass(query_decayed, inner, states, ends, entering):
    before = jnp.cumsum(ends, axis=0) - ends
    states = states + jnp.exp(before)[:, :, :, None] * entering[None]
    out = inner + jnp.einsum("nhtd,nhdv->nhtv", query_decayed, states, precision=highest)
    blocks, heads, rows, width = out.shape
    return out.transpose(0, 2, 1, 3).reshape(blocks * rows, heads, width)


def entering_state(totals, states, index):
    size = totals.shape[0]
    k = jnp.arange(size)
    reached = (k < index)[:, None]
    masked = jnp.where(reached, totals, 0.0)
    after = (k[None, :] > k[:, None]).astype(jnp.float32)
    behind = jnp.sum(after[:, :, None] * masked[None], axis=1)
    factor = jnp.where(reached, jnp.exp(behind), 0.0)
    return jnp.sum(factor[:, :, None] * states.astype(jnp.float32), axis=0)


def head_norm(attention, head_gain, gate):
    inverse_rms = lax.rsqrt(jnp.mean(attention * attention, axis=-1, keepdims=True) + epsilon)
    gate_silu = jax.nn.silu(gate.astype(jnp.float32).reshape(attention.shape))
    mixed_rows = attention * inverse_rms * head_gain * gate_silu
    return mixed_rows.astype(jnp.bfloat16).reshape(attention.shape[0], -1)


def rms_scale(residual, gain_vector):
    as_float = residual.astype(jnp.float32)
    inverse_rms = lax.rsqrt(jnp.mean(as_float * as_float, axis=-1, keepdims=True) + epsilon)
    return (as_float * inverse_rms * gain_vector).astype(jnp.bfloat16)


def route_positions(block_routes, experts):
    flattened = block_routes.reshape(-1)
    amount = flattened.shape[0]
    onehot = flattened[:, None] == jnp.arange(experts, dtype=jnp.int32)[None, :]
    earlier = jnp.tril(jnp.ones((amount, amount), jnp.bfloat16), -1)
    before = jnp.dot(earlier, onehot.astype(jnp.bfloat16), preferred_element_type=jnp.float32)
    ranking = jnp.sum(jnp.where(onehot, before, 0.0), axis=1).astype(jnp.int32)
    return ranking.reshape(block_routes.shape)


def add_all(parts):
    return jnp.sum(parts.astype(jnp.float32), axis=0)


def shards(
    query_first,
    key_first,
    value_first,
    decay_first,
    gate_first,
    norm_first,
    proj_first,
    query_second,
    key_second,
    value_second,
    decay_second,
    gate_second,
    norm_second,
    proj_second,
    residual_in,
    expert_norm,
    route_ids,
    route_weight,
    expert_gate,
    expert_up,
    expert_down,
):
    sp_size, tp_size = lax.axis_size("sp"), lax.axis_size("tp")
    sp_index, tp_index = lax.axis_index("sp"), lax.axis_index("tp")
    projection = jnp.concatenate((proj_first, proj_second), axis=0)
    projection = lax.all_gather(projection, "sp", axis=1, tiled=True)

    first = local_pass(query_first, key_first, value_first, decay_first, KA, VA)
    second = local_pass(query_second, key_second, value_second, decay_second, KB, VB)
    total_first = jnp.sum(first[3], axis=0).reshape(1, -1)
    total_second = jnp.sum(second[3], axis=0).reshape(1, -1)
    totals = jnp.concatenate((total_first, total_second), axis=1)
    totals = jnp.broadcast_to(totals, (8, totals.shape[1]))
    all_totals, all_first, all_second = exchange(
        (
            totals,
            first[4].reshape(-1, VA).astype(jnp.bfloat16),
            second[4].reshape(-1, VB).astype(jnp.bfloat16),
        ),
        "sp",
        sp_size,
        False,
        0,
    )
    cut = total_first.shape[1]
    enter_first = entering_state(all_totals[:, 0, :cut], all_first, sp_index)
    enter_second = entering_state(all_totals[:, 0, cut:], all_second, sp_index)
    attention_first = finish_pass(*first[:4], enter_first.reshape(first[4].shape))
    attention_second = finish_pass(*second[:4], enter_second.reshape(second[4].shape))
    mixed_first = head_norm(attention_first, norm_first, gate_first)
    mixed_second = head_norm(attention_second, norm_second, gate_second)
    mixed_rows = jnp.concatenate((mixed_first, mixed_second), axis=1)
    partial_terms = jnp.dot(mixed_rows, projection, preferred_element_type=jnp.float32)
    block_tokens, top_count = route_ids.shape
    model_width = partial_terms.shape[1]
    own_tokens = block_tokens // tp_size
    (portions,) = exchange(
        (partial_terms.astype(jnp.bfloat16).reshape(tp_size, own_tokens, model_width),),
        "tp",
        tp_size,
        True,
        1,
    )
    residual = (residual_in.astype(jnp.float32) + add_all(portions)).astype(jnp.bfloat16)
    normed = rms_scale(residual, expert_norm)
    (gathered,) = exchange((normed,), "tp", tp_size, False, 2)
    gathered = gathered.reshape(block_tokens, model_width)

    experts = sp_size
    capacity = 2 * top_count * block_tokens // experts
    half = capacity // PAIR
    slots = experts * half
    place = route_positions(route_ids, experts) - lax.rem(tp_index, PAIR) * half
    local = jnp.where((place >= 0) & (place < half), route_ids * half + place, -1)
    numbers = jnp.arange(slots, dtype=jnp.int32)
    chosen, weights = (False, 0.0)
    for c in range(top_count):
        chosen = chosen | (numbers[:, None] == local[None, :, c])
        weights = weights + jnp.where(
            numbers[None, :] == local[:, c, None], route_weight[:, c, None], 0.0
        )
    outgoing = jnp.dot(
        chosen.astype(jnp.bfloat16), gathered, preferred_element_type=jnp.float32
    ).astype(jnp.bfloat16)
    incoming = dispatch(outgoing.reshape(experts, half, model_width), 3)
    incoming = incoming.reshape(-1, model_width)
    gate_part = jnp.dot(incoming, expert_gate[0], preferred_element_type=jnp.float32)
    up_part = jnp.dot(incoming, expert_up[0], preferred_element_type=jnp.float32)
    hidden = (jax.nn.silu(gate_part) * up_part).astype(jnp.bfloat16)
    produced = jnp.dot(hidden, expert_down[0], preferred_element_type=jnp.float32)
    produced = produced.astype(jnp.bfloat16).reshape(PAIR, slots, model_width)
    (halves,) = exchange((produced,), "tp", PAIR, True, 4)
    summed = add_all(halves).astype(jnp.bfloat16).reshape(experts, half, model_width)
    (returned,) = exchange((summed,), "sp", sp_size, True, 5)
    returned = returned.reshape(slots, model_width)
    coarse = weights.astype(jnp.bfloat16)
    fine = (weights - coarse.astype(jnp.float32)).astype(jnp.bfloat16)
    weighted = jnp.dot(coarse, returned, preferred_element_type=jnp.float32)
    weighted = weighted + jnp.dot(fine, returned, preferred_element_type=jnp.float32)
    (shares,) = exchange(
        (weighted.astype(jnp.bfloat16).reshape(tp_size, own_tokens, model_width),),
        "tp",
        tp_size,
        True,
        6,
    )
    return (residual.astype(jnp.float32) + add_all(shares)).astype(jnp.bfloat16)


def solution(mesh):
    in_specs = (
        P("sp", "tp"),
        P("sp", "tp"),
        P("sp", "tp"),
        P("sp", "tp"),
        P("sp", "tp"),
        P(),
        P("tp", "sp"),
        P("sp", "tp"),
        P("sp", "tp"),
        P("sp", "tp"),
        P("sp", "tp"),
        P("sp", "tp"),
        P(),
        P("tp", "sp"),
        P(("sp", "tp"), None),
        P(),
        P("sp", None),
        P("sp", None),
        P("sp", None, "tp"),
        P("sp", None, "tp"),
        P("sp", "tp", None),
    )
    out_specs = P(("sp", "tp"), None)
    return jax.shard_map(shards, mesh=mesh, in_specs=in_specs, out_specs=out_specs, check_vma=False)
```

time: 399 us -> 283 us (0.71)
  Pallas kernels: 0 us -> 197 us
  waiting for transfers between devices: 187 us -> 12 us
  blocking collectives: 104 us -> 0 us
  local copies, waits for them, and re-layouts: 28.2 us -> 8.05 us
  other arithmetic: 25.9 us -> 15.7 us
  starting transfers between devices: 5.83 us -> 0.01 us
  matrix products: 30.3 us -> 35.7 us
    pallas_call x0 -> x7, Pallas kernels: none -> 197 us  [the longest x6 141 us: exchange(): pl.pallas_call(functools.partial(exchange_kernel, axis, span, spread, cou...]
    reduce_scatter x3 -> x0, waiting for transfers between devices: 116 us -> none  [the longest x1 46.7 us: shards(): lax.psum_scatter(partial_terms.astype(jnp.bfloat16), 'tp', scatter_dimens...]
    all_gather x4 -> x0, blocking collectives: 75.9 us -> none  [entering(): lax.all_gather(part.astype(kind), axis)]
    all_gather x3 -> x1, waiting for transfers between devices: 49 us -> 12 us  [shards(): projection = lax.all_gather(projection, 'sp', axis=1, tiled=True)]
    all_to_all x1 -> x0, blocking collectives: 28.1 us -> none  [shards(): lax.all_to_all(own_slots, 'sp', split_axis=0, concat_axis=0, tiled=True)]
    all_to_all x1 -> x0, waiting for transfers between devices: 22 us -> none  [shards(): lax.all_to_all(summed.astype(jnp.bfloat16), 'sp', split_axis=0, concat_ax...]
    gather x3 -> x0, local copies, waits for them, and re-layouts: 15.5 us -> none  [the longest x2 9.48 us: shards(): picked = jnp.take(flat_back, local_index, axis=0)]
    all_to_all x1 -> x0, starting transfers between devices: 5.48 us -> none  [shards(): lax.all_to_all(summed.astype(jnp.bfloat16), 'sp', split_axis=0, concat_ax...]
  transfers between devices with their start and end apart: 7 -> 1, of which waited for: 6 -> 1; matrix products, arithmetic and copies ran while one was open for 7% -> 7% of each run, Pallas kernels for 0% -> 11%
where the time goes in v1:
time: 283 us
  Pallas kernels  197 us (70%)
  matrix products  35.7 us (13%)
  other arithmetic  15.7 us (6%)
  between operations  14 us (5%)
  waiting for transfers between devices  12 us (4%)
  local copies, waits for them, and re-layouts  8.05 us (3%)
    pallas_call x6, Pallas kernels, exchange(): pl.pallas_call(functools.partial(exchange_kernel, axis, span, spread, cou...  141 us
    pallas_call x1, Pallas kernels, dispatch(): pl.pallas_call(functools.partial(dispatch_kernel, size), out_shape=jax.Sh...  56.3 us
    all_gather x1, waiting for transfers between devices, shards(): projection = lax.all_gather(projection, 'sp', axis=1, tiled=True)  12 us
    reduce_sum x3, other arithmetic, add_all(): return jnp.sum(parts.astype(jnp.float32), axis=0)  7.96 us
    dot_general x1, matrix products, shards(): jnp.dot(incoming, expert_up[0], preferred_element_type=jnp.float32)  7.68 us
    dot_general x1, matrix products, shards(): jnp.dot(hidden, expert_down[0], preferred_element_type=jnp.float32)  6.07 us
  transfers between devices with their start and end apart: 1, of which 1 were waited for; matrix products, arithmetic and copies ran while one was open for 7% of the time, Pallas kernels for 11%

profile of v1, /device:TPU:13, one launch (start us, length us, event | category | flops | bytes accessed | tf_op | source)
XLA Modules:
  0.0 282.7 jit_solution(2989451759534517953)
XLA Ops:
  6.5 1.7 pad_maximum_fusion
  8.3 1.2 convolution_bitcast_fusion.1
  9.5 1.1 reshape.506
  10.6 0.4 convolution_bitcast_fusion
  11.0 1.0 reshape.520
  12.1 0.9 reshape.509
  13.0 0.5 broadcast.265
  13.5 0.6 fusion.114
  14.2 0.1 exp.168
  14.3 0.1 exp.170
  14.3 0.1 exp.172
  14.4 0.1 mul.367
  14.5 0.1 reshape.507
  14.6 0.4 fusion.46
  15.0 1.3 fusion.75
  16.3 0.1 multiply_add_fusion
  16.4 0.8 fusion.93
  17.2 0.7 fusion.94.refs_2_
  17.9 0.6 broadcast_in_dim.118.refs_0_
  18.5 31.2 %shard_map.199 = (f32[8,8,256]{2,1,0:T(8,128)}, bf16[8,128,256]{2,1,0:T(8,128)(2,1)}, bf16[8,128,128]{2,1,0:T(8,128)(2,1)}) custom-call(f32[8,256]{1,0:T(8,128)} %broadcast_in_dim.118.refs_0_, bf16[128,256]{1,0:T(8,128)(2,1)} %get-tuple-element.22.refs_1_, bf16[128,128]{1,0:T(8,128)(2,1)} %fusion.94.refs_2_), custom_call_target="tpu_custom_call" | custom-call | tf_op jit(solution)/shard_map/pallas_call | solution.py:68
  49.7 0.9 copy.84
  50.6 0.8 slice.105
  51.4 0.2 mul.388
  51.7 0.6 convolution_multiply_fusion
  52.3 0.3 fusion.79
  52.6 0.1 broadcast_select_fusion
  52.6 0.1 multiply_reduce_fusion.5
  52.8 1.2 multiply_reduce_fusion.1
  54.0 0.6 multiply_reduce_fusion.2
  54.7 0.1 copy.94
  54.8 0.2 copy.86
  55.0 0.2 multiply_reduce_fusion
  55.3 0.4 convolution_multiply_fusion.1
  55.6 0.2 fusion.137
  55.9 0.6 multiply_reduce_fusion.3
  56.5 0.1 rsqrt.31
  56.6 0.1 copy.89
  56.8 0.1 eq.72
  56.9 0.3 fusion.9
  57.3 0.1 sub.58
  57.5 0.1 copy.91
  57.6 0.2 slice_reduce_fusion.1
  57.9 0.3 mul.409
  58.2 0.2 fusion.65
  58.5 12.0 %all-gather.2.cloned.1.call-done = bf16[512,2048]{1,0:T(8,128)(2,1)} async-done(((bf16[512,256]{1,0:T(8,128)(2,1)}), bf16[512,2048]{1,0:T(8,128)(2,1)}) %all-gather.2.cloned.1.call-update) | async-done | bytes 2097168 | tf_op jit(solution)/shard_map/all_gather | solution.py:246
  70.5 3.3 %convolution_convert_fusion.2 = bf16[256,2048]{1,0:T(8,128)(2,1)} fusion(bf16[512,2048]{1,0:T(8,128)(2,1)} %all-gather.2.cloned.1.call-done, bf16[256,256]{1,0:T(8,128)(2,1)S(1)} %get-tuple-element.56, bf16[256,256]{1,0:T(8,128)(2,1)S(1)} %get-tuple-element.55), kind=kOutput, calls=%fused_computation.10 | convolution fusion | flops 537919488 | bytes 3407872 | tf_op jit(solution)/shard_map/dot_general | solution.py:273
  73.8 17.0 %shard_map.200 = bf16[4,64,2048]{2,1,0:T(8,128)(2,1)} custom-call(bf16[4,64,2048]{2,1,0:T(8,128)(2,1)} %bitcast.171), custom_call_target="tpu_custom_call" | custom-call | tf_op jit(solution)/shard_map/pallas_call | solution.py:68
  90.8 1.4 convert_reduce_fusion.1
  92.2 0.2 fusion.12
  92.4 0.8 fusion.14.refs_0_
  93.3 15.7 %shard_map.201 = bf16[4,64,2048]{2,1,0:T(8,128)(2,1)} custom-call(bf16[64,2048]{1,0:T(8,128)(2,1)} %fusion.14.refs_0_), custom_call_target="tpu_custom_call" | custom-call | tf_op jit(solution)/shard_map/pallas_call | solution.py:68
  108.9 3.3 %convolution_convert_fusion.1 = bf16[512,2048]{1,0:T(8,128)(2,1)} fusion(bf16[256,2048]{1,0:T(8,128)(2,1)} %bitcast.172, s32[256]{0:T(256)S(1)} %get-tuple-element.15, s32[256]{0:T(256)S(1)} %get-tuple-element.14), kind=kOutput, calls=%fused_computation.7 | convolution fusion | flops 538312704 | bytes 3147776 | tf_op jit(solution)/shard_map/dot_general | solution.py:302
  112.2 56.3 %shard_map.202 = bf16[2,8,64,2048]{3,2,1,0:T(8,128)(2,1)} custom-call(bf16[8,64,2048]{2,1,0:T(8,128)(2,1)} %bitcast.167), custom_call_target="tpu_custom_call" | custom-call | tf_op jit(solution)/shard_map/pallas_call | solution.py:131
  168.6 7.7 %fusion.1 = f32[1024,896]{1,0:T(8,128)S(1)} fusion(bf16[1024,2048]{1,0:T(8,128)(2,1)} %bitcast.168, bf16[1,2048,896]{2,1,0:T(8,128)(2,1)} %param.40), kind=kOutput, calls=%fused_computation.2 | convolution fusion | flops 3758096384 | bytes 11534336 | tf_op jit(solution)/shard_map/dot_general | solution.py:308
  176.3 4.7 %multiply_convert_fusion = bf16[1024,896]{1,0:T(8,128)(2,1)S(1)} fusion(f32[1024,896]{1,0:T(8,128)S(1)} %fusion.1, bf16[1024,2048]{1,0:T(8,128)(2,1)S(1)} %bitcast.169, bf16[1,2048,896]{2,1,0:T(8,128)(2,1)S(1)} %copy-done.14), kind=kOutput, calls=%fused_computation.6 | convolution fusion | flops 3763601408 | bytes 13369344 | tf_op jit(solution)/shard_map/dot_general | solution.py:307
  181.1 6.1 %convolution_convert_fusion = bf16[1024,2048]{1,0:T(8,128)(2,1)} fusion(bf16[1024,896]{1,0:T(8,128)(2,1)S(1)} %multiply_convert_fusion, bf16[1,896,2048]{2,1,0:T(8,128)(2,1)S(1)} %copy-done.15), kind=kOutput, calls=%fused_computation | convolution fusion | flops 3760193536 | bytes 9699328 | tf_op jit(solution)/shard_map/dot_general | solution.py:310
  187.2 8.3 %shard_map.203 = bf16[2,512,2048]{2,1,0:T(8,128)(2,1)} custom-call(bf16[2,512,2048]{2,1,0:T(8,128)(2,1)} %bitcast.170), custom_call_target="tpu_custom_call" | custom-call | tf_op jit(solution)/shard_map/pallas_call | solution.py:68
  195.5 5.1 %reduce_sum.134 = bf16[512,2048]{1,0:T(8,128)(2,1)} reduce(bf16[2,512,2048]{2,1,0:T(8,128)(2,1)} %shard_map.203, bf16[]{:T(256)} %constant.62.clone.1), dimensions={0}, to_apply=%region_13.14 | reduce | flops 1048576 | bytes 6291458 | tf_op jit(solution)/shard_map/reduce_sum | solution.py:217
  200.6 52.1 %shard_map.204 = bf16[8,64,2048]{2,1,0:T(8,128)(2,1)} custom-call(bf16[8,64,2048]{2,1,0:T(8,128)(2,1)} %bitcast.166), custom_call_target="tpu_custom_call" | custom-call | tf_op jit(solution)/shard_map/pallas_call | solution.py:68
  252.7 2.5 fusion.70
  255.2 1.8 fusion.5
  257.1 16.5 %shard_map.205 = bf16[4,64,2048]{2,1,0:T(8,128)(2,1)} custom-call(bf16[4,64,2048]{2,1,0:T(8,128)(2,1)} %bitcast.173), custom_call_target="tpu_custom_call" | custom-call | tf_op jit(solution)/shard_map/pallas_call | solution.py:68
  273.6 1.4 convert_reduce_fusion
  275.1 0.8 fusion.15
  (59 shorter events, 0.4 us)
Async XLA Ops:
  6.5 8.5 %copy-start = (bf16[256,256]{1,0:T(8,128)(2,1)S(1)}, bf16[256,256]{1,0:T(8,128)(2,1)}, u32[]{:S(2)}) copy-start(bf16[256,256]{1,0:T(8,128)(2,1)} %param.23) | copy-start | bytes 393220
  6.5 44.9 %copy-start.8 = (bf16[256,128]{1,0:T(8,128)(2,1)S(1)}, bf16[256,128]{1,0:T(8,128)(2,1)}, u32[]{:S(2)}) copy-start(bf16[256,128]{1,0:T(8,128)(2,1)} %param.28) | copy-start | bytes 196612
  6.5 63.9 %all-gather.2.cloned.1.call-start = ((), (), s32[]{:S(2)}) async-start(), calls=%async_computation | async-start | bytes 2359296 | tf_op jit(solution)/shard_map/all_gather | solution.py:246
  16.4 38.8 %copy-start.9 = (bf16[256,128]{1,0:T(8,128)(2,1)S(1)}, bf16[256,128]{1,0:T(8,128)(2,1)}, u32[]{:S(2)}) copy-start(bf16[256,128]{1,0:T(8,128)(2,1)} %param.21) | copy-start | bytes 196612
  16.4 38.9 %copy-start.5 = (bf16[256,128]{1,0:T(8,128)(2,1)S(1)}, bf16[256,128]{1,0:T(8,128)(2,1)}, u32[]{:S(2)}) copy-start(bf16[256,128]{1,0:T(8,128)(2,1)} %param.22) | copy-start | bytes 196612
  49.7 5.3 %copy-start.3 = (bf16[8,128,256]{2,1,0:T(8,128)(2,1)S(1)}, bf16[8,128,256]{2,1,0:T(8,128)(2,1)}, u32[]{:S(2)}) copy-start(bf16[8,128,256]{2,1,0:T(8,128)(2,1)} %get-tuple-element.9) | copy-start | bytes 1572868
  51.6 5.0 %copy-start.11 = (s32[256,2]{0,1:T(2,128)S(1)}, s32[256,2]{0,1:T(2,128)}, u32[]{:S(2)}) copy-start(s32[256,2]{0,1:T(2,128)} %param.37) | copy-start | bytes 6148
  54.0 3.8 %copy-start.16 = (f32[128]{0:T(128)S(1)}, f32[128]{0:T(128)}, u32[]{:S(2)}) copy-start(f32[128]{0:T(128)} %param.33) | copy-start | bytes 1540
  54.0 3.9 %copy-start.12 = (f32[256,2]{0,1:T(2,128)S(1)}, f32[256,2]{0,1:T(2,128)}, u32[]{:S(2)}) copy-start(f32[256,2]{0,1:T(2,128)} %param.38) | copy-start | bytes 6148
  54.0 4.2 %copy-start.6 = (bf16[256,256]{1,0:T(8,128)(2,1)S(1)}, bf16[256,256]{1,0:T(8,128)(2,1)}, u32[]{:S(2)}) copy-start(bf16[256,256]{1,0:T(8,128)(2,1)} %param.25) | copy-start | bytes 393220
  54.0 4.2 %copy-start.7 = (bf16[256,256]{1,0:T(8,128)(2,1)S(1)}, bf16[256,256]{1,0:T(8,128)(2,1)}, u32[]{:S(2)}) copy-start(bf16[256,256]{1,0:T(8,128)(2,1)} %param.32) | copy-start | bytes 393220
  54.0 4.2 %copy-start.13 = (f32[256]{0:T(256)S(1)}, f32[256]{0:T(256)}, u32[]{:S(2)}) copy-start(f32[256]{0:T(256)} %param.26) | copy-start | bytes 3076
  58.5 33.8 %copy-start.4 = (bf16[64,2048]{1,0:T(8,128)(2,1)S(1)}, bf16[64,2048]{1,0:T(8,128)(2,1)}, u32[]{:S(2)}) copy-start(bf16[64,2048]{1,0:T(8,128)(2,1)} %param.35) | copy-start | bytes 786436
  70.5 22.0 %copy-start.10 = (f32[2048]{0:T(1024)S(1)}, f32[2048]{0:T(1024)}, u32[]{:S(2)}) copy-start(f32[2048]{0:T(1024)} %param.36) | copy-start | bytes 24580
  168.6 7.7 %copy-start.2 = (bf16[2,8,64,2048]{3,2,1,0:T(8,128)(2,1)S(1)}, bf16[2,8,64,2048]{3,2,1,0:T(8,128)(2,1)}, u32[]{:S(2)}) copy-start(bf16[2,8,64,2048]{3,2,1,0:T(8,128)(2,1)} %shard_map.202) | copy-start | bytes 12582916
  168.6 7.7 %copy-start.14 = (bf16[1,2048,896]{2,1,0:T(8,128)(2,1)S(1)}, bf16[1,2048,896]{2,1,0:T(8,128)(2,1)}, u32[]{:S(2)}) copy-start(bf16[1,2048,896]{2,1,0:T(8,128)(2,1)} %param.39) | copy-start | bytes 11010052
  176.3 4.8 %copy-start.15 = (bf16[1,896,2048]{2,1,0:T(8,128)(2,1)S(1)}, bf16[1,896,2048]{2,1,0:T(8,128)(2,1)}, u32[]{:S(2)}) copy-start(bf16[1,896,2048]{2,1,0:T(8,128)(2,1)} %param.41) | copy-start | bytes 11010052
  252.7 2.6 copy-start.1
Sparse Core Ops, SparseCore 0:
  9.4 61.0 all-gather.1

commit v2 on v1

--- a/solution.py
+++ b/solution.py
@@ -78,64 +78,161 @@
     )(*arrays)
 
 
-def dispatch_kernel(size, source, target, send_sems, recv_sems, pair_send, pair_recv):
-    half = lax.rem(lax.axis_index("tp"), PAIR)
-    sibling = group_member("tp", PAIR, 1)[2]
-    peers = [group_member("sp", size, step) for step in range(1, size)]
-    greet([peer[2] for peer in peers] + [sibling])
-    copies, forwards = [], []
-    for step, (me, other, device) in enumerate(peers, 1):
-        copy = pltpu.make_async_remote_copy(
-            src_ref=source.at[other],
-            dst_ref=target.at[half, me],
-            send_sem=send_sems.at[step],
-            recv_sem=recv_sems.at[step],
-            device_id=device,
-            device_id_type=MESH,
-        )
-        copy.start()
-        copies.append(copy)
-    me = lax.axis_index("sp")
-    own = pltpu.make_async_remote_copy(
-        src_ref=source.at[me],
-        dst_ref=target.at[half, me],
-        send_sem=pair_send.at[0],
-        recv_sem=pair_recv.at[0],
-        device_id=sibling,
+def tp_member(across, sibling):
+    size, me = lax.axis_size("tp"), lax.axis_index("tp")
+    seat = lax.rem(me, PAIR)
+    base = lax.rem(me - seat + across * PAIR, size)
+    return base + (lax.rem(seat + 1, PAIR) if sibling else seat)
+
+
+def remote(source, target, sems, index, device):
+    return pltpu.make_async_remote_copy(
+        src_ref=source,
+        dst_ref=target,
+        send_sem=sems[0].at[index],
+        recv_sem=sems[1].at[index],
+        device_id=device,
         device_id_type=MESH,
     )
-    own.start()
-    forwards.append(own)
-    target[half, me] = source[me]
-    for step in range(1, size):
-        copies[step - 1].wait_recv()
-        origin = lax.rem(me - step + size, size)
-        forward = pltpu.make_async_remote_copy(
-            src_ref=target.at[half, origin],
-            dst_ref=target.at[half, origin],
-            send_sem=pair_send.at[step],
-            recv_sem=pair_recv.at[step],
-            device_id=sibling,
-            device_id_type=MESH,
-        )
-        forward.start()
-        forwards.append(forward)
-    for copy in copies:
+
+
+def gather_kernel(size, pairs, spread, source, target, *sems):
+    sp_sems, pair_sems, far_sems = sems[:2], sems[2:4], sems[4:]
+    me, mine = lax.axis_index("sp"), lax.axis_index("tp")
+    sibling = {"tp": tp_member(0, True)}
+    far = [{"tp": tp_member(across, False)} for across in range(1, pairs)]
+    peers = [group_member("sp", size, step) for step in range(1, size)] if spread else []
+    greet([peer[2] for peer in peers] + [sibling] + far)
+    copies = []
+    for step, (_, other, device) in enumerate(peers, 1):
+        copies.append(remote(source.at[other], target.at[mine, me], sp_sems, step, device))
+        copies[-1].start()
+    passed, distant = [], []
+    for step in range(size):
+        if spread:
+            origin = lax.rem(me - step + size, size)
+        else:
+            origin = step
+        own = step == 0 or not spread
+        if not own:
+            copies[step - 1].wait_recv()
+        block = source.at[origin] if own else target.at[mine, origin]
+        for across in range(1, pairs):
+            copy = remote(
+                block, target.at[mine, origin], far_sems, (across, step), far[across - 1]
+            )
+            copy.start()
+            distant.append((copy, tp_member(pairs - across, False), origin, across, step))
+        copy = remote(block, target.at[mine, origin], pair_sems, (0, step), sibling)
+        copy.start()
+        passed.append(copy)
+        if own:
+            target[mine, origin] = source[origin]
+    for copy, sender, origin, across, step in distant:
+        copy.wait_recv()
+        block = target.at[sender, origin]
+        again = remote(block, block, pair_sems, (across, step), sibling)
+        again.start()
+        passed.append(again)
+    for copy in copies + [item[0] for item in distant]:
         copy.wait_send()
-    for forward in forwards:
-        forward.wait()
-
-
-def dispatch(outgoing, number):
-    size = outgoing.shape[0]
+    for copy in passed:
+        copy.wait()
+
+
+def gather_tp(blocks, spread, number):
+    size, tp = blocks.shape[0], lax.axis_size("tp")
+    pairs = tp // PAIR
     return pl.pallas_call(
-        functools.partial(dispatch_kernel, size),
-        out_shape=jax.ShapeDtypeStruct((PAIR,) + outgoing.shape, outgoing.dtype),
+        functools.partial(gather_kernel, size, pairs, spread),
+        out_shape=jax.ShapeDtypeStruct((tp,) + blocks.shape, blocks.dtype),
         in_specs=[VMEM],
         out_specs=VMEM,
-        scratch_shapes=[pltpu.SemaphoreType.DMA((size,)) for _ in range(4)],
+        scratch_shapes=[pltpu.SemaphoreType.DMA((size,))] * 2
+        + [pltpu.SemaphoreType.DMA((pairs, size))] * 4,
         compiler_params=pltpu.CompilerParams(collective_id=number, has_side_effects=True),
-    )(outgoing)
+    )(blocks)
+
+
+def reduce_kernel(size, pairs, spread, source, target, near, paired, arrived, *rest):
+    done = rest[0] if spread else None
+    sems = rest[1:] if spread else rest
+    pair_sems, far_sems, sp_sems = sems[:2], sems[2:4], sems[4:]
+    me = lax.axis_index("sp")
+    sibling = {"tp": tp_member(0, True)}
+    far = [{"tp": tp_member(across, False)} for across in range(1, pairs)]
+    peers = [group_member("sp", size, step) for step in range(1, size)] if spread else []
+    greet([peer[2] for peer in peers] + [sibling] + far)
+    order = [lax.rem(me + k + 1, size) if spread else k for k in range(size)]
+    hops = list(range(1, pairs)) + [0]
+    first = {}
+    for k in range(size):
+        for across in hops:
+            copy = remote(
+                source.at[tp_member(across, True), order[k]],
+                near.at[across, order[k]],
+                pair_sems,
+                (across, k),
+                sibling,
+            )
+            copy.start()
+            first[k, across] = copy
+    second = {}
+    for k in range(size):
+        for across in hops:
+            first[k, across].wait_recv()
+            total = source[tp_member(across, False), order[k]].astype(jnp.float32)
+            total = total + near[across, order[k]].astype(jnp.float32)
+            paired[across, order[k]] = total.astype(paired.dtype)
+        for across in range(1, pairs):
+            copy = remote(
+                paired.at[across, order[k]],
+                arrived.at[across, order[k]],
+                far_sems,
+                (across, k),
+                far[across - 1],
+            )
+            copy.start()
+            second[k, across] = copy
+    third = []
+    for k in range(size):
+        total = paired[0, order[k]].astype(jnp.float32)
+        for across in range(1, pairs):
+            second[k, across].wait_recv()
+            total = total + arrived[across, order[k]].astype(jnp.float32)
+        if not spread:
+            target[order[k]] = total
+        elif k == size - 1:
+            target[me] = total.astype(target.dtype)
+        else:
+            done[order[k]] = total.astype(done.dtype)
+            copy = remote(done.at[order[k]], target.at[me], sp_sems, k, peers[k][2])
+            copy.start()
+            third.append(copy)
+    for copy in list(first.values()) + list(second.values()):
+        copy.wait_send()
+    for copy in third:
+        copy.wait()
+
+
+def reduce_tp(blocks, spread, number):
+    tp, size, rows, width = blocks.shape
+    pairs = tp // PAIR
+    kept = pltpu.VMEM((pairs, size, rows, width), jnp.bfloat16)
+    done = [pltpu.VMEM((size, rows, width), jnp.bfloat16)] if spread else []
+    return pl.pallas_call(
+        functools.partial(reduce_kernel, size, pairs, spread),
+        out_shape=jax.ShapeDtypeStruct(
+            (size, rows, width), jnp.bfloat16 if spread else jnp.float32
+        ),
+        in_specs=[VMEM],
+        out_specs=VMEM,
+        scratch_shapes=[kept] * 3
+        + done
+        + [pltpu.SemaphoreType.DMA((pairs, size))] * 4
+        + [pltpu.SemaphoreType.DMA((size,))] * 2,
+        compiler_params=pltpu.CompilerParams(collective_id=number, has_side_effects=True),
+    )(blocks)
 
 
 def local_pass(queries, key_rows, values, decay_factors, key_width, value_width):
@@ -211,10 +308,6 @@
     before = jnp.dot(earlier, onehot.astype(jnp.bfloat16), preferred_element_type=jnp.float32)
     ranking = jnp.sum(jnp.where(onehot, before, 0.0), axis=1).astype(jnp.int32)
     return ranking.reshape(block_routes.shape)
-
-
-def add_all(parts):
-    return jnp.sum(parts.astype(jnp.float32), axis=0)
 
 
 def shards(
@@ -242,26 +335,27 @@
 ):
     sp_size, tp_size = lax.axis_size("sp"), lax.axis_size("tp")
     sp_index, tp_index = lax.axis_index("sp"), lax.axis_index("tp")
-    projection = jnp.concatenate((proj_first, proj_second), axis=0)
-    projection = lax.all_gather(projection, "sp", axis=1, tiled=True)
-
     first = local_pass(query_first, key_first, value_first, decay_first, KA, VA)
     second = local_pass(query_second, key_second, value_second, decay_second, KB, VB)
     total_first = jnp.sum(first[3], axis=0).reshape(1, -1)
     total_second = jnp.sum(second[3], axis=0).reshape(1, -1)
     totals = jnp.concatenate((total_first, total_second), axis=1)
     totals = jnp.broadcast_to(totals, (8, totals.shape[1]))
-    all_totals, all_first, all_second = exchange(
+    all_totals, all_first, all_second, *columns = exchange(
         (
             totals,
             first[4].reshape(-1, VA).astype(jnp.bfloat16),
             second[4].reshape(-1, VB).astype(jnp.bfloat16),
+            proj_first,
+            proj_second,
         ),
         "sp",
         sp_size,
         False,
         0,
     )
+    columns = [part.transpose(1, 0, 2).reshape(part.shape[1], -1) for part in columns]
+    projection = jnp.concatenate(columns, axis=0)
     cut = total_first.shape[1]
     enter_first = entering_state(all_totals[:, 0, :cut], all_first, sp_index)
     enter_second = entering_state(all_totals[:, 0, cut:], all_second, sp_index)
@@ -274,24 +368,20 @@
     block_tokens, top_count = route_ids.shape
     model_width = partial_terms.shape[1]
     own_tokens = block_tokens // tp_size
-    (portions,) = exchange(
-        (partial_terms.astype(jnp.bfloat16).reshape(tp_size, own_tokens, model_width),),
-        "tp",
-        tp_size,
-        True,
-        1,
-    )
-    residual = (residual_in.astype(jnp.float32) + add_all(portions)).astype(jnp.bfloat16)
+    by_owner = (tp_size, PAIR, own_tokens // PAIR, model_width)
+    mixture = reduce_tp(partial_terms.astype(jnp.bfloat16).reshape(by_owner), False, 1)
+    mixture = mixture.reshape(own_tokens, model_width)
+    residual = (residual_in.astype(jnp.float32) + mixture).astype(jnp.bfloat16)
     normed = rms_scale(residual, expert_norm)
-    (gathered,) = exchange((normed,), "tp", tp_size, False, 2)
+    gathered = gather_tp(normed.reshape(by_owner[1:]), False, 2)
     gathered = gathered.reshape(block_tokens, model_width)
 
     experts = sp_size
     capacity = 2 * top_count * block_tokens // experts
-    half = capacity // PAIR
-    slots = experts * half
-    place = route_positions(route_ids, experts) - lax.rem(tp_index, PAIR) * half
-    local = jnp.where((place >= 0) & (place < half), route_ids * half + place, -1)
+    quarter = capacity // tp_size
+    slots = experts * quarter
+    place = route_positions(route_ids, experts) - tp_index * quarter
+    local = jnp.where((place >= 0) & (place < quarter), route_ids * quarter + place, -1)
     numbers = jnp.arange(slots, dtype=jnp.int32)
     chosen, weights = (False, 0.0)
     for c in range(top_count):
@@ -302,29 +392,22 @@
     outgoing = jnp.dot(
         chosen.astype(jnp.bfloat16), gathered, preferred_element_type=jnp.float32
     ).astype(jnp.bfloat16)
-    incoming = dispatch(outgoing.reshape(experts, half, model_width), 3)
+    incoming = gather_tp(outgoing.reshape(experts, quarter, model_width), True, 3)
     incoming = incoming.reshape(-1, model_width)
     gate_part = jnp.dot(incoming, expert_gate[0], preferred_element_type=jnp.float32)
     up_part = jnp.dot(incoming, expert_up[0], preferred_element_type=jnp.float32)
     hidden = (jax.nn.silu(gate_part) * up_part).astype(jnp.bfloat16)
     produced = jnp.dot(hidden, expert_down[0], preferred_element_type=jnp.float32)
-    produced = produced.astype(jnp.bfloat16).reshape(PAIR, slots, model_width)
-    (halves,) = exchange((produced,), "tp", PAIR, True, 4)
-    summed = add_all(halves).astype(jnp.bfloat16).reshape(experts, half, model_width)
-    (returned,) = exchange((summed,), "sp", sp_size, True, 5)
+    produced = produced.astype(jnp.bfloat16).reshape(tp_size, experts, quarter, model_width)
+    returned = reduce_tp(produced, True, 4)
     returned = returned.reshape(slots, model_width)
     coarse = weights.astype(jnp.bfloat16)
     fine = (weights - coarse.astype(jnp.float32)).astype(jnp.bfloat16)
     weighted = jnp.dot(coarse, returned, preferred_element_type=jnp.float32)
     weighted = weighted + jnp.dot(fine, returned, preferred_element_type=jnp.float32)
-    (shares,) = exchange(
-        (weighted.astype(jnp.bfloat16).reshape(tp_size, own_tokens, model_width),),
-        "tp",
-        tp_size,
-        True,
-        6,
-    )
-    return (residual.astype(jnp.float32) + add_all(shares)).astype(jnp.bfloat16)
+    combined = reduce_tp(weighted.astype(jnp.bfloat16).reshape(by_owner), False, 5)
+    combined = combined.reshape(own_tokens, model_width)
+    return (residual.astype(jnp.float32) + combined).astype(jnp.bfloat16)
 
 
 def solution(mesh):

time: 283 us -> 249 us (0.88)
  between operations: 14 us -> 0.57 us
  waiting for transfers between devices: 12 us -> 0 us
  Pallas kernels: 197 us -> 191 us
  other arithmetic: 15.7 us -> 11.2 us
    pallas_call x6 -> x1, Pallas kernels: 141 us -> 71.3 us  [exchange(): pl.pallas_call(functools.partial(exchange_kernel, axis, span, spread, cou...]
    pallas_call x1 -> x5, Pallas kernels: 56.3 us -> 120 us  [the longest x3 70.2 us: reduce_tp(): pl.pallas_call(functools.partial(reduce_kernel, size, pairs, spread), out...]
    all_gather x1 -> x0, waiting for transfers between devices: 12 us -> none  [shards(): projection = lax.all_gather(projection, 'sp', axis=1, tiled=True)]
    reduce_sum x4 -> x0, other arithmetic: 7.98 us -> none  [the longest x3 7.96 us: add_all(): return jnp.sum(parts.astype(jnp.float32), axis=0)]
  transfers between devices with their start and end apart: 1 -> 0, of which waited for: 1 -> 0; matrix products, arithmetic and copies ran while one was open for 7% -> 0% of each run, Pallas kernels for 11% -> 0%
where the time goes in v2:
time: 249 us; the launch traced here: 248 us
  Pallas kernels  191 us (77%)
  matrix products  34.5 us (14%)
  other arithmetic  11.2 us (4%)
  local copies, waits for them, and re-layouts  10.7 us (4%)
    pallas_call x1, Pallas kernels, exchange(): pl.pallas_call(functools.partial(exchange_kernel, axis, span, spread, cou...  71.3 us
    pallas_call x3, Pallas kernels, reduce_tp(): pl.pallas_call(functools.partial(reduce_kernel, size, pairs, spread), out...  70.2 us
    pallas_call x2, Pallas kernels, gather_tp(): pl.pallas_call(functools.partial(gather_kernel, size, pairs, spread), out...  49.7 us
    dot_general x1, matrix products, shards(): jnp.dot(incoming, expert_up[0], preferred_element_type=jnp.float32)  7.5 us
    dot_general x1, matrix products, shards(): jnp.dot(hidden, expert_down[0], preferred_element_type=jnp.float32)  6.05 us

profile of v2, /device:TPU:13, one launch (start us, length us, event | category | flops | bytes accessed | tf_op | source)
XLA Modules:
  0.0 248.2 jit_solution(18302834398684022188)
XLA Ops:
  0.0 1.1 reshape.518
  1.2 0.4 convolution_bitcast_fusion
  1.6 1.0 reshape.536
  2.6 0.9 reshape.521
  3.5 0.4 fusion.47
  3.9 0.5 broadcast.264
  4.5 0.7 fusion.118
  5.1 0.1 multiply_add_fusion
  5.3 0.1 exp.168
  5.3 0.1 exp.170
  5.4 0.1 exp.172
  5.5 0.1 mul.367
  5.6 0.7 fusion.98.refs_2_
  6.3 1.2 convolution_bitcast_fusion.1
  7.5 0.4 fusion.69
  8.0 0.8 fusion.97
  8.8 0.1 reshape.519
  8.9 0.6 broadcast_in_dim.118.refs_0_
  9.5 71.3 %shard_map.199 = (f32[8,8,256]{2,1,0:T(8,128)}, bf16[8,128,256]{2,1,0:T(8,128)(2,1)}, bf16[8,128,128]{2,1,0:T(8,128)(2,1)}, bf16[8,256,256]{2,1,0:T(8,128)(2,1)}, bf16[8,256,256]{2,1,0:T(8,128)(2,1)}) custom-call(f32[8,256]{1,0:T(8,128)} %broadcast_in_dim.118.refs_0_, bf16[128,256]{1,0:T(8,128)(2,1)} %get-tuple-element.29.refs_1_, ...), custom_call_target="tpu_custom_call" | custom-call | tf_op jit(solution)/shard_map/pallas_call | solution.py:68
  80.8 0.9 copy.94
  81.7 0.8 slice.105
  82.4 0.1 broadcast_select_fusion
  82.5 0.1 multiply_reduce_fusion.5
  82.6 0.1 exponential_select_fusion.1
  82.7 1.2 multiply_reduce_fusion.1
  83.9 0.2 mul.388
  84.1 0.0 copy-start.12
  84.1 0.6 convolution_multiply_fusion
  84.7 0.3 fusion.73
  85.0 0.6 multiply_reduce_fusion.2
  85.6 0.1 copy.106
  85.8 0.3 mul.409
  86.1 0.2 copy.96
  86.3 1.3 multiply_reduce_fusion
  87.7 0.9 convert_multiply_fusion.7
  88.6 1.2 convolution_multiply_fusion.1
  89.8 0.3 fusion.143
  90.1 1.6 multiply_reduce_fusion.3
  91.7 0.1 rsqrt.31
  91.7 0.7 broadcast_bitcast_fusion
  92.4 1.2 fusion.60
  93.6 1.5 copy.99
  95.1 0.5 copy.100
  95.7 3.0 %convolution_convert_fusion.1 = bf16[256,2048]{1,0:T(8,128)(2,1)} fusion(bf16[256,2048]{0,1:T(8,128)(2,1)S(1)} %bitcast.189, bf16[256,2048]{0,1:T(8,128)(2,1)} %bitcast.188, bf16[256,256]{1,0:T(8,128)(2,1)S(1)} %get-tuple-element.62, bf16[256,256]{1,0:T(8,128)(2,1)S(1)} %get-tuple-element.61), kind=kOutput, calls=%fused_computation.8 | convolution fusion | flops 542113792 | bytes 3407872 | tf_op jit(solution)/shard_map/dot_general | solution.py:367
  98.7 12.2 %shard_map.200 = f32[2,32,2048]{2,1,0:T(8,128)} custom-call(bf16[4,2,32,2048]{3,2,1,0:T(8,128)(2,1)} %bitcast.185), custom_call_target="tpu_custom_call" | custom-call | tf_op jit(solution)/shard_map/pallas_call | solution.py:223
  110.9 1.2 fusion.15
  112.2 0.8 fusion.17
  113.0 11.8 %shard_map.201 = bf16[4,2,32,2048]{3,2,1,0:T(8,128)(2,1)} custom-call(bf16[2,32,2048]{2,1,0:T(8,128)(2,1)} %bitcast.184), custom_call_target="tpu_custom_call" | custom-call | tf_op jit(solution)/shard_map/pallas_call | solution.py:146
  124.8 0.1 copy.101
  125.0 0.1 eq.72
  125.1 0.3 fusion.12
  125.5 0.1 sub.58
  125.7 0.1 copy.103
  125.8 0.2 slice_reduce_fusion.1
  126.0 2.6 %convolution_convert_fusion.2 = bf16[256,2048]{1,0:T(8,128)(2,1)} fusion(bf16[256,2048]{1,0:T(8,128)(2,1)} %bitcast.180, s32[256]{0:T(256)S(1)} %get-tuple-element.19, s32[256]{0:T(256)S(1)} %get-tuple-element.18), kind=kOutput, calls=%fused_computation.10 | convolution fusion | flops 269156352 | bytes 2099200 | tf_op jit(solution)/shard_map/dot_general | solution.py:392
  128.7 37.9 %shard_map.202 = bf16[4,8,32,2048]{3,2,1,0:T(8,128)(2,1)} custom-call(bf16[8,32,2048]{2,1,0:T(8,128)(2,1)} %bitcast.176), custom_call_target="tpu_custom_call" | custom-call | tf_op jit(solution)/shard_map/pallas_call | solution.py:146
  166.6 7.5 %fusion.1 = f32[1024,896]{1,0:T(8,128)S(1)} fusion(bf16[1024,2048]{1,0:T(8,128)(2,1)} %bitcast.177, bf16[1,2048,896]{2,1,0:T(8,128)(2,1)} %param.40), kind=kOutput, calls=%fused_computation.2 | convolution fusion | flops 3758096384 | bytes 11534336 | tf_op jit(solution)/shard_map/dot_general | solution.py:398
  174.2 4.7 %multiply_convert_fusion = bf16[1024,896]{1,0:T(8,128)(2,1)S(1)} fusion(f32[1024,896]{1,0:T(8,128)S(1)} %fusion.1, bf16[1024,2048]{1,0:T(8,128)(2,1)S(1)} %bitcast.178, bf16[1,2048,896]{2,1,0:T(8,128)(2,1)S(1)} %copy-done.13), kind=kOutput, calls=%fused_computation.6 | convolution fusion | flops 3763601408 | bytes 13369344 | tf_op jit(solution)/shard_map/dot_general | solution.py:397
  178.9 6.1 %convolution_convert_fusion = bf16[1024,2048]{1,0:T(8,128)(2,1)} fusion(bf16[1024,896]{1,0:T(8,128)(2,1)S(1)} %multiply_convert_fusion, bf16[1,896,2048]{2,1,0:T(8,128)(2,1)S(1)} %copy-done.14), kind=kOutput, calls=%fused_computation | convolution fusion | flops 3760193536 | bytes 9699328 | tf_op jit(solution)/shard_map/dot_general | solution.py:400
  185.0 45.7 %shard_map.203 = bf16[8,32,2048]{2,1,0:T(8,128)(2,1)} custom-call(bf16[4,8,32,2048]{3,2,1,0:T(8,128)(2,1)} %bitcast.179), custom_call_target="tpu_custom_call" | custom-call | tf_op jit(solution)/shard_map/pallas_call | solution.py:223
  230.7 1.8 fusion.93
  232.6 1.5 fusion.5
  234.1 12.2 %shard_map.204 = f32[2,32,2048]{2,1,0:T(8,128)} custom-call(bf16[4,2,32,2048]{3,2,1,0:T(8,128)(2,1)} %bitcast.181), custom_call_target="tpu_custom_call" | custom-call | tf_op jit(solution)/shard_map/pallas_call | solution.py:223
  246.4 1.8 fusion.18
  (49 shorter events, 0.3 us)
Async XLA Ops:
  0.0 7.5 %copy-start = (bf16[256,256]{1,0:T(8,128)(2,1)S(1)}, bf16[256,256]{1,0:T(8,128)(2,1)}, u32[]{:S(2)}) copy-start(bf16[256,256]{1,0:T(8,128)(2,1)} %param.23) | copy-start | bytes 393220
  0.0 7.5 %copy-start.7 = (bf16[256,128]{1,0:T(8,128)(2,1)S(1)}, bf16[256,128]{1,0:T(8,128)(2,1)}, u32[]{:S(2)}) copy-start(bf16[256,128]{1,0:T(8,128)(2,1)} %param.22) | copy-start | bytes 196612
  0.0 83.8 %copy-start.8 = (bf16[256,128]{1,0:T(8,128)(2,1)S(1)}, bf16[256,128]{1,0:T(8,128)(2,1)}, u32[]{:S(2)}) copy-start(bf16[256,128]{1,0:T(8,128)(2,1)} %param.28) | copy-start | bytes 196612
  84.1 0.6 copy-start.5
  84.1 8.3 %copy-start.12 = (f32[256]{0:T(256)S(1)}, f32[256]{0:T(256)}, u32[]{:S(2)}) copy-start(f32[256]{0:T(256)} %param.26) | copy-start | bytes 3076
  85.0 8.6 %copy-start.4 = (bf16[8,256,256]{2,1,0:T(8,128)(2,1)S(1)}, bf16[8,256,256]{2,1,0:T(8,128)(2,1)}, u32[]{:S(2)}) copy-start(bf16[8,256,256]{2,1,0:T(8,128)(2,1)} %get-tuple-element.13) | copy-start | bytes 3145732
  86.1 9.0 %copy-start.3 = (bf16[8,256,256]{2,1,0:T(8,128)(2,1)S(1)}, bf16[8,256,256]{2,1,0:T(8,128)(2,1)}, u32[]{:S(2)}) copy-start(bf16[8,256,256]{2,1,0:T(8,128)(2,1)} %get-tuple-element.14) | copy-start | bytes 3145732
  95.6 15.3 %copy-start.6 = (bf16[64,2048]{1,0:T(8,128)(2,1)S(1)}, bf16[64,2048]{1,0:T(8,128)(2,1)}, u32[]{:S(2)}) copy-start(bf16[64,2048]{1,0:T(8,128)(2,1)} %param.35) | copy-start | bytes 786436
  95.7 16.5 %copy-start.9 = (f32[2048]{0:T(1024)S(1)}, f32[2048]{0:T(1024)}, u32[]{:S(2)}) copy-start(f32[2048]{0:T(1024)} %param.36) | copy-start | bytes 24580
  95.7 29.2 %copy-start.10 = (s32[256,2]{0,1:T(2,128)S(1)}, s32[256,2]{0,1:T(2,128)}, u32[]{:S(2)}) copy-start(s32[256,2]{0,1:T(2,128)} %param.37) | copy-start | bytes 6148
  166.6 7.5 %copy-start.2 = (bf16[4,8,32,2048]{3,2,1,0:T(8,128)(2,1)S(1)}, bf16[4,8,32,2048]{3,2,1,0:T(8,128)(2,1)}, u32[]{:S(2)}) copy-start(bf16[4,8,32,2048]{3,2,1,0:T(8,128)(2,1)} %shard_map.202) | copy-start | bytes 12582916
  166.6 7.5 %copy-start.13 = (bf16[1,2048,896]{2,1,0:T(8,128)(2,1)S(1)}, bf16[1,2048,896]{2,1,0:T(8,128)(2,1)}, u32[]{:S(2)}) copy-start(bf16[1,2048,896]{2,1,0:T(8,128)(2,1)} %param.39) | copy-start | bytes 11010052
  174.2 4.8 %copy-start.14 = (bf16[1,896,2048]{2,1,0:T(8,128)(2,1)S(1)}, bf16[1,896,2048]{2,1,0:T(8,128)(2,1)}, u32[]{:S(2)}) copy-start(bf16[1,896,2048]{2,1,0:T(8,128)(2,1)} %param.41) | copy-start | bytes 11010052
  185.0 45.7 %copy-start.11 = (f32[256,2]{0,1:T(2,128)S(1)}, f32[256,2]{0,1:T(2,128)}, u32[]{:S(2)}) copy-start(f32[256,2]{0,1:T(2,128)} %param.38) | copy-start | bytes 6148
  230.7 1.9 copy-start.1
